TPU v7x, 32 devices: a whole 2x2x4 slice. The times are simulated.
32 devices in a mesh: grp: 2 (over x), tp: 16 (over z, y, core).
Axes of the slice: x: 2, y: 2, z: 4, core: 2. Of those that a mesh axis runs over, the one named last changes fastest.
Arguments:
- tokens: bfloat16 [128, 2048], P('grp'), parts along dimension 0, may hold values from -6 to 6
- norm_gain: float32 [2, 2048], replicated, may hold values from 0.1 to 1.9
- query_weight: bfloat16 [2, 2048, 2048], P(None, 'tp'), may hold values from -0.125 to 0.125
- key_weight: bfloat16 [2, 2048, 2048], P(None, 'tp'), may hold values from -0.125 to 0.125
- value_weight: bfloat16 [2, 2048, 2048], P(None, 'tp'), may hold values from -0.125 to 0.125
- outgate_weight: bfloat16 [2, 2048, 2048], P(None, 'tp'), may hold values from -0.125 to 0.125
- gate_weight: bfloat16 [2, 2048, 16], replicated, may hold values from -0.125 to 0.125
- forget_bias: float32 [2, 8], replicated, may hold values from 0 to 4
- proj_weight: bfloat16 [2, 2048, 2048], P(None, 'tp'), may hold values from -0.125 to 0.125
- cell_state: float32 [2, 128, 2048, 256], P(None, 'grp', 'tp'), parts along dimension 1, may hold values from -0.3 to 0.3
- normalizer: float32 [2, 128, 2048], P(None, 'grp', 'tp'), parts along dimension 1, may hold values from -0.3 to 0.3
- stabilizer: float32 [2, 128, 8], P(None, 'grp'), parts along dimension 1, may hold values from -2 to 2
Outputs:
- mixed: bfloat16 [128, 2048], P('grp', 'tp'), parts along dimension 0
- new_cell: float32 [2, 128, 2048, 256], P(None, 'grp', 'tp'), parts along dimension 1
- new_normalizer: float32 [2, 128, 2048], P(None, 'grp', 'tp'), parts along dimension 1
- new_stabilizer: float32 [2, 128, 8], P(None, 'grp'), parts along dimension 1
There are 2 independent parts, one for each index of `grp`. A program takes and returns all parts, laid end to end along the dimension named above; an argument that names none is the same for every part. Nothing has to cross between parts.
All inputs are finite; a program needn't handle non-finite values.
Results may differ from a plain program's by a relative error of at most 0.025.
Values may be sent and summed in bfloat16 or wider, within the bound.
A program may use at most 64 MiB of HBM per device.

v0:
```python
import jax
import jax.numpy as jnp
from jax import lax
from jax.sharding import PartitionSpec as P

D = 2048
DH = 256
LAYERS = 2


epsilon = 1e-06


def from_partner(value, axis, apart):
    mask = 2**apart
    pairs = [(source, source ^ mask) for source in range(lax.axis_size(axis))]
    return lax.ppermute(value, axis, pairs)


def project(normed, weight):
    return lax.dot_general(
        normed, weight, (((1,), (1,)), ((), ())), preferred_element_type=jnp.float32
    )


def split_pieces(value):
    high = lax.optimization_barrier(value.astype(jnp.bfloat16))
    rest = value - high.astype(jnp.float32)
    middle = lax.optimization_barrier(rest.astype(jnp.bfloat16))
    lowest = (rest - middle.astype(jnp.float32)).astype(jnp.bfloat16)
    return jnp.stack([high, middle, lowest], axis=1)


def join_pieces(pieces):
    return jnp.sum(pieces.astype(jnp.float32), axis=-1)


def combine_halves(mine, theirs, lower):
    return jnp.where(
        lower, jnp.concatenate([mine, theirs], axis=1), jnp.concatenate([theirs, mine], axis=1)
    )


def one_cell(
    current,
    gain,
    w_query,
    w_key,
    w_value,
    w_outgate,
    w_gates,
    bias_forget,
    w_proj,
    cell,
    norm_vec,
    stab,
):
    heads = D // DH
    ncols = w_query.shape[0]
    group = DH // ncols
    device = lax.axis_index("tp")
    head = device // group
    cur_f = current.astype(jnp.float32)
    normed = (
        cur_f * lax.rsqrt(jnp.mean(cur_f * cur_f, axis=-1, keepdims=True) + epsilon) * gain
    ).astype(jnp.bfloat16)
    query = project(normed, w_query).astype(jnp.bfloat16)
    keys = (project(normed, w_key) * DH ** (-0.5)).astype(jnp.bfloat16)
    values = project(normed, w_value).astype(jnp.bfloat16)
    outgate = project(normed, w_outgate).astype(jnp.bfloat16)
    gates = jnp.dot(normed, w_gates, preferred_element_type=jnp.float32)
    in_gate = gates[:, :heads]
    log_forget = jax.nn.log_sigmoid(gates[:, heads:] + bias_forget)
    new_stab = jnp.maximum(log_forget + stab, in_gate)
    decay = jnp.exp(log_forget + stab - new_stab)
    weight_in = jnp.exp(in_gate - new_stab)
    select = (jnp.arange(heads) == head).astype(jnp.float32)
    my_decay = jnp.sum(decay * select, axis=-1)
    my_weight = jnp.sum(weight_in * select, axis=-1)
    my_stab = jnp.sum(new_stab * select, axis=-1)
    new_norm = my_decay[:, None] * norm_vec + my_weight[:, None] * keys.astype(jnp.float32)
    den_part = jnp.sum(query.astype(jnp.float32) * new_norm, axis=-1)
    q_head, k_head = (query, keys)
    denom = den_part
    for bit in range(group.bit_length() - 1):
        other_q, other_k, other_pieces = from_partner(
            (q_head, k_head, split_pieces(denom)), "tp", bit
        )
        lower = device // 2**bit % 2 == 0
        q_head = combine_halves(q_head, other_q, lower)
        k_head = combine_halves(k_head, other_k, lower)
        denom = denom + join_pieces(other_pieces)
    outer = values.astype(jnp.float32)[:, :, None] * k_head.astype(jnp.float32)[:, None, :]
    new_cell = my_decay[:, None, None] * cell + my_weight[:, None, None] * outer
    numer = jnp.einsum(
        "bk,bek->be", q_head.astype(jnp.float32), new_cell, precision=lax.Precision.HIGHEST
    )
    readout = numer / jnp.maximum(jnp.abs(denom), jnp.exp(-my_stab))[:, None]
    branch = (jax.nn.sigmoid(outgate.astype(jnp.float32)) * readout).astype(jnp.bfloat16)
    summed = project(lax.all_gather(branch, "tp", axis=1, tiled=True), w_proj)
    own_input = lax.dynamic_slice_in_dim(cur_f, device * ncols, ncols, 1)
    result = (own_input + summed).astype(jnp.bfloat16)
    return (result, new_cell, new_norm, new_stab)


def body(
    tokens,
    norm_gain,
    query_weight,
    key_weight,
    value_weight,
    outgate_weight,
    gate_weight,
    forget_bias,
    proj_weight,
    cell_state,
    normalizer,
    stabilizer,
):
    current = tokens
    cells = []
    norms = []
    stabs = []
    result = tokens
    for layer in range(LAYERS):
        result, new_cell, new_norm, new_stab = one_cell(
            current,
            norm_gain[layer],
            query_weight[layer],
            key_weight[layer],
            value_weight[layer],
            outgate_weight[layer],
            gate_weight[layer],
            forget_bias[layer],
            proj_weight[layer],
            cell_state[layer],
            normalizer[layer],
            stabilizer[layer],
        )
        cells.append(new_cell)
        norms.append(new_norm)
        stabs.append(new_stab)
        if layer + 1 < LAYERS:
            current = lax.all_gather(result, "tp", axis=1, tiled=True)
    return (result, jnp.stack(cells), jnp.stack(norms), jnp.stack(stabs))


def solution(mesh):
    return jax.shard_map(
        body,
        mesh=mesh,
        in_specs=(
            P("grp", None),
            P(),
            P(None, "tp", None),
            P(None, "tp", None),
            P(None, "tp", None),
            P(None, "tp", None),
            P(),
            P(),
            P(None, "tp", None),
            P(None, "grp", "tp", None),
            P(None, "grp", "tp"),
            P(None, "grp", None),
        ),
        out_specs=(
            P("grp", "tp"),
            P(None, "grp", "tp", None),
            P(None, "grp", "tp"),
            P(None, "grp", None),
        ),
        check_vma=False,
    )
```

profile of v0, /device:TPU:0, one launch (start us, length us, event | category | flops | bytes accessed | tf_op | source)
XLA Modules:
  0.0 111.6 jit_solution(17831152566984168210)
XLA Ops:
  0.6 1.1 multiply_reduce_fusion.1
  1.7 0.8 fusion.88
  2.6 0.0 copy-start.2
  2.6 1.5 %fusion.20 = bf16[64,128]{1,0:T(8,128)(2,1)S(1)} fusion(bf16[2,128,2048]{2,1,0:T(8,128)(2,1)} %param.15, f32[2048]{0:T(1024)S(1)} %bitcast.105, f32[64]{0:T(128)S(1)} %add_rsqrt_fusion.1, bf16[64,2048]{1,0:T(8,128)(2,1)} %param.12), kind=kOutput, calls=%fused_computation.27 | convolution fusion | flops 34095104 | bytes 811264 | tf_op jit(solution)/shard_map/dot_general | solution.py:21
  4.1 0.6 collective-permute-start.1
  4.6 1.5 %convolution_convert_fusion.4 = bf16[64,128]{1,0:T(8,128)(2,1)S(1)} fusion(bf16[2,128,2048]{2,1,0:T(8,128)(2,1)} %param.14, f32[2048]{0:T(1024)S(1)} %bitcast.106, f32[64]{0:T(128)S(1)} %add_rsqrt_fusion.1, bf16[64,2048]{1,0:T(8,128)(2,1)} %param.12), kind=kOutput, calls=%fused_computation.44 | convolution fusion | flops 34086912 | bytes 811264 | tf_op jit(solution)/shard_map/dot_general | solution.py:21
  6.1 0.0 copy-start.3
  6.1 0.1 collective-permute-start
  6.2 0.8 slice_bitcast_fusion
  7.0 1.2 %fusion.62 = f32[64,16]{0,1:T(8,128)S(1)} fusion(bf16[2,2048,16]{1,2,0:T(8,128)(2,1)} %param.18, f32[2048]{0:T(1024)S(1)} %bitcast.107, f32[64]{0:T(128)S(1)} %add_rsqrt_fusion.1, bf16[64,2048]{1,0:T(8,128)(2,1)} %param.12), kind=kOutput, calls=%fused_computation.80 | convolution fusion | flops 4718592 | bytes 340224 | tf_op jit(solution)/shard_map/dot_general | solution.py:71
  8.2 0.8 fusion.84
  9.0 0.1 multiply_reduce_fusion.7
  9.1 1.0 fusion.74
  10.1 0.5 collective-permute-start.2
  10.6 1.0 convert_element_type.132
  11.6 0.0 copy-start.9
  11.6 1.5 %fusion.32 = f32[64,128]{1,0:T(8,128)S(1)} fusion(bf16[2,128,2048]{2,1,0:T(8,128)(2,1)} %param.16, f32[2048]{0:T(1024)S(1)} %bitcast.108, f32[64]{0:T(128)S(1)} %add_rsqrt_fusion.1, bf16[64,2048]{1,0:T(8,128)(2,1)} %param.12), kind=kOutput, calls=%fused_computation.43 | convolution fusion | flops 34095104 | bytes 827648 | tf_op jit(solution)/shard_map/dot_general | solution.py:21
  13.2 0.0 copy-start.5
  13.2 0.0 copy-start.10
  13.2 0.0 collective-permute-done.2
  13.3 0.0 collective-permute-done
  13.3 0.0 collective-permute-done.1
  13.3 0.0 copy-start.7
  13.3 0.0 copy-start.4
  13.4 0.0 copy-start
  13.4 7.6 %fusion.4 = f32[64,1,128]{2,1,0:T(1,128)S(1)} fusion(f32[2,64,128,256]{3,2,1,0:T(8,128)} %param.21, f32[64,256]{1,0:T(8,128)S(1)} %fusion.69, f32[64,128]{1,0:T(8,128)S(1)} %fusion.32, f32[64]{0:T(128)S(1)} %get-tuple-element.8, f32[64]{0:T(128)S(1)} %get-tuple-element.9, bf16[64,256,1]{1,0,2:T(8,128)(2,1)S(1)} %fusion.68), kind=kOutput, calls=%fused_computation.6 | convolution fusion | flops 33554432 | bytes 8552960 | tf_op jit(solution)/shard_map/bk,bek->be/dot_general | solution.py:95
  21.0 0.0 copy-done.2
  21.0 1.4 %fusion.39 = bf16[64,128]{1,0:T(8,128)(2,1)S(1)} fusion(bf16[2,128,2048]{2,1,0:T(8,128)(2,1)} %param.17, f32[64,128]{1,0:T(8,128)S(1)} %bitcast.115, f32[64]{0:T(128)S(1)} %exponential_maximum_fusion.1, f32[2048]{0:T(1024)S(1)} %bitcast.109, f32[64]{0:T(128)S(1)} %add_rsqrt_fusion.1, bf16[64,2048]{1,0:T(8,128)(2,1)S(1)} %copy-done.2), kind=kOutput, calls=%fused_computation.52 | convolution fusion | flops 34144256 | bytes 844288 | tf_op jit(solution)/shard_map/dot_general | solution.py:21
  22.4 23.4 %all_gather.9 = bf16[64,2048]{1,0:T(8,128)(2,1)S(1)} all-gather(bf16[64,128]{1,0:T(8,128)(2,1)S(1)} %fusion.39), channel_id=1, replica_groups=mesh['grp'=2,'tp'=16] {'tp'}, dimensions={1}, use_global_device_ids=true | all-gather | bytes 278528 | tf_op jit(solution)/shard_map/all_gather | solution.py:100
  45.8 0.3 fusion.21
  46.1 18.2 %all_gather.10 = bf16[64,2048]{1,0:T(8,128)(2,1)S(1)} all-gather(bf16[64,128]{1,0:T(8,128)(2,1)S(1)} %fusion.21), channel_id=1, replica_groups=mesh['grp'=2,'tp'=16] {'tp'}, dimensions={1}, use_global_device_ids=true | all-gather | bytes 278528 | tf_op jit(solution)/shard_map/all_gather | solution.py:144
  64.2 0.2 multiply_reduce_fusion
  64.4 0.0 copy-done.11
  64.4 0.2 fusion.60
  64.7 0.0 copy-done.9
  64.7 0.3 convolution_convert_fusion.1
  65.0 0.0 copy-done.10
  65.0 0.3 fusion.22
  65.4 1.4 %fusion.24 = f32[64,128]{1,0:T(8,128)S(1)} fusion(bf16[2,128,2048]{2,1,0:T(8,128)(2,1)} %param.16, f32[2048]{0:T(1024)S(1)} %bitcast.103, f32[64]{0:T(128)S(1)} %add_rsqrt_fusion, bf16[64,2048]{1,0:T(8,128)(2,1)S(1)} %all_gather.10), kind=kOutput, calls=%fused_computation.32 | convolution fusion | flops 34095104 | bytes 827648 | tf_op jit(solution)/shard_map/dot_general | solution.py:21
  66.8 0.0 copy-start.6
  66.8 0.0 copy-done.7
  66.8 0.1 fusion.85
  66.9 0.1 multiply_reduce_fusion.4
  67.0 0.4 collective-permute-start.4
  67.3 0.2 collective-permute-start.3
  67.5 0.2 fusion.75
  67.7 0.4 collective-permute-start.5
  68.2 0.6 pad_maximum_fusion.1
  68.8 0.6 pad_maximum_fusion.2
  69.4 0.8 convert_element_type.152
  70.2 0.0 collective-permute-done.5
  70.2 0.5 exponential_maximum_fusion
  70.8 0.0 collective-permute-done.4
  70.8 0.0 copy-done
  70.8 5.1 %multiply_add_fusion.1 = (f32[1,64,128,256]{3,2,1,0:T(8,128)S(1)}, f32[1,64,128,256]{3,2,1,0:T(8,128)S(1)}) fusion(f32[2,64,128,256]{3,2,1,0:T(8,128)S(1)} %copy-done, f32[64,256]{1,0:T(8,128)S(1)} %fusion.69, f32[64,128]{1,0:T(8,128)} %copy-done.5, f32[64]{0:T(128)S(1)} %get-tuple-element.8, f32[64]{0:T(128)S(1)} %get-tuple-element.9, ...), kind=kLoop, calls=%fused_computation.8 | loop fusion | flops 16777216 | bytes 33752064 | tf_op jit(solution)/shard_map/add | solution.py:94
  75.9 0.0 copy-start.8
  75.9 0.0 copy-start.13
  75.9 0.0 collective-permute-done.3
  76.0 6.3 %fusion.1 = f32[64,1,128]{2,1,0:T(1,128)S(1)} fusion(f32[2,64,128,256]{3,2,1,0:T(8,128)S(1)} %copy-done, f32[64,256]{1,0:T(8,128)S(1)} %fusion.71, f32[64,128]{1,0:T(8,128)} %copy-done.6, f32[64]{0:T(128)S(1)} %get-tuple-element.6, f32[64]{0:T(128)S(1)} %get-tuple-element.5, bf16[64,256,1]{1,0,2:T(8,128)(2,1)S(1)} %fusion.70), kind=kOutput, calls=%fused_computation.3 | convolution fusion | flops 33554432 | bytes 8553472 | tf_op jit(solution)/shard_map/bk,bek->be/dot_general | solution.py:95
  82.3 0.0 copy-done.13
  82.3 1.5 %fusion.31 = bf16[64,128]{1,0:T(8,128)(2,1)S(1)} fusion(bf16[2,128,2048]{2,1,0:T(8,128)(2,1)} %param.17, f32[64,128]{1,0:T(8,128)S(1)} %bitcast.114, f32[64]{0:T(128)S(1)} %copy-done.8, f32[2048]{0:T(1024)S(1)} %bitcast.104, f32[64]{0:T(128)S(1)} %copy-done.13, bf16[64,2048]{1,0:T(8,128)(2,1)} %copy-done.1), kind=kOutput, calls=%fused_computation.41 | convolution fusion | flops 34144256 | bytes 844288 | tf_op jit(solution)/shard_map/dot_general | solution.py:21
  83.8 19.5 %all_gather.11 = bf16[64,2048]{1,0:T(8,128)(2,1)S(1)} all-gather(bf16[64,128]{1,0:T(8,128)(2,1)S(1)} %fusion.31), channel_id=1, replica_groups=mesh['grp'=2,'tp'=16] {'tp'}, dimensions={1}, use_global_device_ids=true | all-gather | bytes 278528 | tf_op jit(solution)/shard_map/all_gather | solution.py:100
  103.3 1.9 %fusion.23 = bf16[64,128]{1,0:T(8,128)(2,1)} fusion(bf16[64,2048]{1,0:T(8,128)(2,1)S(1)} %all_gather.11, bf16[2,128,2048]{2,1,0:T(8,128)(2,1)} %param.20, f32[64,2048]{1,0:T(8,128)} %convert_element_type.152, s32[]{:T(128)S(6)} %select_n.56), kind=kOutput, calls=%fused_computation.30 | convolution fusion | flops 33570816 | bytes 835588 | tf_op jit(solution)/shard_map/dot_general | solution.py:21
  105.2 6.4 %pad_maximum_fusion = f32[2,64,128,256]{3,2,1,0:T(8,128)} fusion(f32[1,64,128,256]{3,2,1,0:T(8,128)S(1)} %get-tuple-element.15, f32[1,64,128,256]{3,2,1,0:T(8,128)S(1)} %get-tuple-element.14), kind=kLoop, calls=%fused_computation | loop fusion | flops 4194304 | bytes 33554432 | tf_op jit(solution)/shard_map/stack | solution.py:145
  (28 shorter events, 0.2 us)
Async XLA Ops:
  2.6 18.4 %copy-start.2 = (bf16[64,2048]{1,0:T(8,128)(2,1)S(1)}, bf16[64,2048]{1,0:T(8,128)(2,1)}, u32[]{:S(2)}) copy-start(bf16[64,2048]{1,0:T(8,128)(2,1)} %param.12) | copy-start | bytes 786436
  4.1 9.2 %collective-permute-start.1 = (bf16[64,128]{1,0:T(8,128)(2,1)S(1)}, bf16[64,128]{1,0:T(8,128)(2,1)S(1)}, u32[]{:S(2)}, u32[]{:S(2)}) collective-permute-start(bf16[64,128]{1,0:T(8,128)(2,1)S(1)} %fusion.20), channel_id=1, source_target_pairs={{0,1},{1,0},{2,3},{3,2},{4,5},{5,4},{6,7},{7,6},{8,9},{9,8},{10,11... | collective-permute-start | bytes 49160 | tf_op jit(solution)/shard_map/ppermute | solution.py:17
  6.1 39.7 %copy-start.3 = (bf16[2,128,2048]{2,1,0:T(8,128)(2,1)S(1)}, bf16[2,128,2048]{2,1,0:T(8,128)(2,1)}, u32[]{:S(2)}) copy-start(bf16[2,128,2048]{2,1,0:T(8,128)(2,1)} %param.20) | copy-start | bytes 3145732
  6.1 7.1 %collective-permute-start = (bf16[64,128]{1,0:T(8,128)(2,1)S(1)}, bf16[64,128]{1,0:T(8,128)(2,1)S(1)}, u32[]{:S(2)}, u32[]{:S(2)}) collective-permute-start(bf16[64,128]{1,0:T(8,128)(2,1)S(1)} %convolution_convert_fusion.4), channel_id=1, source_target_pairs={{0,1},{1,0},{2,3},{3,2},{4,5},{5,4},{6,7},{7,6},{8,9},{9,8},{10,11... | collective-permute-start | bytes 49160 | tf_op jit(solution)/shard_map/ppermute | solution.py:17
  10.1 3.2 %collective-permute-start.2 = (bf16[64,3]{0,1:T(4,128)(2,1)S(1)}, bf16[64,3]{0,1:T(4,128)(2,1)S(1)}, u32[]{:S(2)}, u32[]{:S(2)}) collective-permute-start(bf16[64,3]{0,1:T(4,128)(2,1)S(1)} %pad_maximum_fusion.3), channel_id=1, source_target_pairs={{0,1},{1,0},{2,3},{3,2},{4,5},{5,4},{6,7},{7,6},{8,9},{9,8},{10,11... | collective-permute-start | bytes 1160 | tf_op jit(solution)/shard_map/ppermute | solution.py:17
  10.6 53.8 %copy-start.11 = (bf16[2,2048,16]{1,2,0:T(8,128)(2,1)S(1)}, bf16[2,2048,16]{1,2,0:T(8,128)(2,1)}, u32[]{:S(2)}) copy-start(bf16[2,2048,16]{1,2,0:T(8,128)(2,1)} %param.18) | copy-start | bytes 393220
  11.6 53.0 %copy-start.9 = (bf16[2,128,2048]{2,1,0:T(8,128)(2,1)S(1)}, bf16[2,128,2048]{2,1,0:T(8,128)(2,1)}, u32[]{:S(2)}) copy-start(bf16[2,128,2048]{2,1,0:T(8,128)(2,1)} %param.14) | copy-start | bytes 3145732
  13.2 52.2 %copy-start.5 = (f32[64,128]{1,0:T(8,128)}, f32[64,128]{1,0:T(8,128)S(1)}, u32[]{:S(2)}) copy-start(f32[64,128]{1,0:T(8,128)S(1)} %fusion.32) | copy-start | bytes 98308
  13.2 51.8 %copy-start.10 = (bf16[2,128,2048]{2,1,0:T(8,128)(2,1)S(1)}, bf16[2,128,2048]{2,1,0:T(8,128)(2,1)}, u32[]{:S(2)}) copy-start(bf16[2,128,2048]{2,1,0:T(8,128)(2,1)} %param.15) | copy-start | bytes 3145732
  13.3 53.5 %copy-start.7 = (f32[2,64,8]{1,2,0:T(8,128)S(1)}, f32[2,64,8]{1,2,0:T(8,128)}, u32[]{:S(2)}) copy-start(f32[2,64,8]{1,2,0:T(8,128)} %param.23) | copy-start | bytes 12292
  13.3 54.2 %copy-start.4 = (f32[2,64,128]{2,1,0:T(8,128)S(1)}, f32[2,64,128]{2,1,0:T(8,128)}, u32[]{:S(2)}) copy-start(f32[2,64,128]{2,1,0:T(8,128)} %param.22) | copy-start | bytes 196612
  13.4 57.4 %copy-start = (f32[2,64,128,256]{3,2,1,0:T(8,128)S(1)}, f32[2,64,128,256]{3,2,1,0:T(8,128)}, u32[]{:S(2)}) copy-start(f32[2,64,128,256]{3,2,1,0:T(8,128)} %param.21) | copy-start | bytes 50331652
  64.2 6.5 %copy-start.1 = (bf16[64,2048]{1,0:T(8,128)(2,1)}, bf16[64,2048]{1,0:T(8,128)(2,1)S(1)}, u32[]{:S(2)}) copy-start(bf16[64,2048]{1,0:T(8,128)(2,1)S(1)} %all_gather.10) | copy-start | bytes 786436
  64.4 3.1 %copy-start.12 = (f32[64]{0:T(128)}, f32[64]{0:T(128)S(1)}, u32[]{:S(2)}) copy-start(f32[64]{0:T(128)S(1)} %add_rsqrt_fusion) | copy-start | bytes 772
  66.8 9.1 %copy-start.6 = (f32[64,128]{1,0:T(8,128)}, f32[64,128]{1,0:T(8,128)S(1)}, u32[]{:S(2)}) copy-start(f32[64,128]{1,0:T(8,128)S(1)} %fusion.24) | copy-start | bytes 98308
  67.0 3.8 %collective-permute-start.4 = (bf16[64,128]{1,0:T(8,128)(2,1)S(1)}, bf16[64,128]{1,0:T(8,128)(2,1)S(1)}, u32[]{:S(2)}, u32[]{:S(2)}) collective-permute-start(bf16[64,128]{1,0:T(8,128)(2,1)S(1)} %fusion.22), channel_id=1, source_target_pairs={{0,1},{1,0},{2,3},{3,2},{4,5},{5,4},{6,7},{7,6},{8,9},{9,8},{10,11... | collective-permute-start | bytes 49160 | tf_op jit(solution)/shard_map/ppermute | solution.py:17
  67.3 8.6 %collective-permute-start.3 = (bf16[64,128]{1,0:T(8,128)(2,1)S(1)}, bf16[64,128]{1,0:T(8,128)(2,1)S(1)}, u32[]{:S(2)}, u32[]{:S(2)}) collective-permute-start(bf16[64,128]{1,0:T(8,128)(2,1)S(1)} %convolution_convert_fusion.1), channel_id=1, source_target_pairs={{0,1},{1,0},{2,3},{3,2},{4,5},{5,4},{6,7},{7,6},{8,9},{9,8},{10,11... | collective-permute-start | bytes 49160 | tf_op jit(solution)/shard_map/ppermute | solution.py:17
  67.7 2.5 %collective-permute-start.5 = (bf16[64,3]{0,1:T(4,128)(2,1)S(1)}, bf16[64,3]{0,1:T(4,128)(2,1)S(1)}, u32[]{:S(2)}, u32[]{:S(2)}) collective-permute-start(bf16[64,3]{0,1:T(4,128)(2,1)S(1)} %pad_maximum_fusion.4), channel_id=1, source_target_pairs={{0,1},{1,0},{2,3},{3,2},{4,5},{5,4},{6,7},{7,6},{8,9},{9,8},{10,11... | collective-permute-start | bytes 1160 | tf_op jit(solution)/shard_map/ppermute | solution.py:17
  75.9 6.4 %copy-start.8 = (f32[64]{0:T(128)S(1)}, f32[64]{0:T(128)}, u32[]{:S(2)}) copy-start(f32[64]{0:T(128)} %exponential_maximum_fusion) | copy-start | bytes 772
  75.9 6.4 %copy-start.13 = (f32[64]{0:T(128)S(1)}, f32[64]{0:T(128)}, u32[]{:S(2)}) copy-start(f32[64]{0:T(128)} %copy-done.12) | copy-start | bytes 772
where the time goes:
time: 112 us
  blocking collectives  61 us (54%)
  matrix products  27.1 us (24%)
  other arithmetic  18.6 us (17%)
  starting transfers between devices  2.11 us (2%)
  local copies, waits for them, and re-layouts  1.66 us (1%)
    all_gather x2, blocking collectives, one_cell(): summed = project(lax.all_gather(branch, 'tp', axis=1, tiled=True), w_proj)  42.9 us
    all_gather x1, blocking collectives, body(): current = lax.all_gather(result, 'tp', axis=1, tiled=True)  18.2 us
    dot_general x2, matrix products, one_cell(): jnp.einsum('bk,bek->be', q_head.astype(jnp.float32), new_cell, precision=...  13.9 us
    dot_general x10, matrix products, project(): lax.dot_general(normed, weight, (((1,), (1,)), ((), ())), preferred_eleme...  11.7 us
    another operation x7, other arithmetic, body(): return (result, jnp.stack(cells), jnp.stack(norms), jnp.stack(stabs))  9.6 us
    add x1, other arithmetic, one_cell(): new_cell = my_decay[:, None, None] * cell + my_weight[:, None, None] * outer  5.09 us
  transfers between devices with their start and end apart: 6, of which 0 were waited for; matrix products, arithmetic and copies ran while one was open for 14% of the time, Pallas kernels for 0%

commit v1 on v0

--- a/solution.py
+++ b/solution.py
@@ -1,6 +1,10 @@
+import functools
+
 import jax
 import jax.numpy as jnp
 from jax import lax
+from jax.experimental import pallas as pl
+from jax.experimental.pallas import tpu as pltpu
 from jax.sharding import PartitionSpec as P
 
 D = 2048
@@ -145,9 +149,343 @@
     return (result, jnp.stack(cells), jnp.stack(norms), jnp.stack(stabs))
 
 
+NT = (((1,), (1,)), ((), ()))
+CELL_CHUNKS = 4
+
+
+def fused_kernel(
+    n,
+    group,
+    tokens,
+    norm_gain,
+    w_query,
+    w_key,
+    w_value,
+    w_outgate,
+    w_gates,
+    bias_forget,
+    w_proj,
+    cell,
+    norm_vec,
+    stab,
+    mixed,
+    cell_buf,
+    new_norm,
+    new_stab,
+    wv_buf,
+    key_buf,
+    decay_buf,
+    tok_buf,
+    gain_buf,
+    weights,
+    gate_buf,
+    bias_buf,
+    stab_buf,
+    norm_buf,
+    pair_buf,
+    branch_buf,
+    result_buf,
+    numer_buf,
+    small_sem,
+    weight_sem,
+    cell_sem,
+    norm_send,
+    norm_recv,
+    pair_send,
+    pair_recv,
+    gather_send,
+    gather_recv,
+):
+    layers, batch, ncols, dh = cell.shape
+    width = tokens.shape[1]
+    heads = stab.shape[1]
+    rows = batch // CELL_CHUNKS
+    me = lax.axis_index("tp")
+    place = lax.rem(me, group)
+    first = me - place
+    head = lax.div(me, group)
+    barrier = pltpu.get_barrier_semaphore()
+    for i in range(1, n):
+        pl.semaphore_signal(
+            barrier,
+            inc=1,
+            device_id={"tp": lax.rem(me + i, n)},
+            device_id_type=pl.DeviceIdType.MESH,
+        )
+
+    def fetch(source, target, sem):
+        copy = pltpu.make_async_copy(source, target, sem)
+        copy.start()
+        return copy
+
+    small = [
+        fetch(source, target, small_sem.at[i])
+        for i, (source, target) in enumerate(
+            [
+                (tokens, tok_buf),
+                (norm_gain, gain_buf),
+                (w_gates, gate_buf),
+                (bias_forget, bias_buf),
+                (stab, stab_buf),
+            ]
+        )
+    ]
+    norm_copy = fetch(norm_vec, norm_buf.at[place], small_sem.at[5])
+    names = [w_query, w_key, w_value, w_outgate, w_proj]
+    weight_copies = [[None] * 5 for _ in range(layers)]
+    cell_copies = [[None] * CELL_CHUNKS for _ in range(layers)]
+    for layer in range(layers):
+        for i in range(4):
+            weight_copies[layer][i] = fetch(
+                names[i].at[layer],
+                weights.at[layer, pl.ds(i * ncols, ncols)],
+                weight_sem.at[layer, i],
+            )
+        for c in range(CELL_CHUNKS):
+            part = pl.ds(c * rows, rows)
+            cell_copies[layer][c] = fetch(
+                cell.at[layer, part], cell_buf.at[layer, part], cell_sem.at[layer, c]
+            )
+        weight_copies[layer][4] = fetch(
+            names[4].at[layer],
+            weights.at[layer, pl.ds(4 * ncols, ncols)],
+            weight_sem.at[layer, 4],
+        )
+
+    def to_group(source, send, recv):
+        copies = []
+        for i in range(1, group):
+            copy = pltpu.make_async_remote_copy(
+                src_ref=source.at[place],
+                dst_ref=source.at[place],
+                send_sem=send.at[i],
+                recv_sem=recv.at[i],
+                device_id={"tp": first + lax.rem(place + i, group)},
+                device_id_type=pl.DeviceIdType.MESH,
+            )
+            copy.start()
+            copies.append(copy)
+        return copies
+
+    def finish_group(copies, source, recv):
+        for i, copy in enumerate(copies, 1):
+            origin = lax.rem(place + group - i, group)
+            pltpu.make_async_copy(source.at[origin], source.at[origin], recv.at[i]).wait()
+            copy.wait_send()
+
+    def to_all(buffer, send, recv):
+        copies = []
+        for i in range(1, n):
+            copy = pltpu.make_async_remote_copy(
+                src_ref=buffer.at[me],
+                dst_ref=buffer.at[me],
+                send_sem=send.at[i],
+                recv_sem=recv.at[i],
+                device_id={"tp": lax.rem(me + i, n)},
+                device_id_type=pl.DeviceIdType.MESH,
+            )
+            copy.start()
+            copies.append(copy)
+        return copies
+
+    def finish_all(copies, buffer, recv):
+        for i, copy in enumerate(copies, 1):
+            origin = lax.rem(me + n - i, n)
+            pltpu.make_async_copy(buffer.at[origin], buffer.at[origin], recv.at[i]).wait()
+            copy.wait_send()
+
+    for copy in small:
+        copy.wait()
+    norm_copies = None
+    own = tok_buf[:, pl.ds(pl.multiple_of(me * ncols, ncols), ncols)].astype(jnp.float32)
+    for layer in range(layers):
+        if layer == 0:
+            current = tok_buf[...].astype(jnp.float32)
+        else:
+            current = jnp.concatenate(
+                [result_buf[layer - 1, d] for d in range(n)], axis=1
+            ).astype(jnp.float32)
+        mean = jnp.sum(current * current, axis=-1, keepdims=True) * (1.0 / width)
+        normed = (current * lax.rsqrt(mean + epsilon) * gain_buf[pl.ds(layer, 1), :]).astype(
+            jnp.bfloat16
+        )
+        for i in range(4):
+            weight_copies[layer][i].wait()
+        both = lax.dot_general(
+            normed, weights[layer, : 2 * ncols], NT, preferred_element_type=jnp.float32
+        )
+        query = both[:, :ncols].astype(jnp.bfloat16)
+        key = (both[:, ncols:] * dh ** (-0.5)).astype(jnp.bfloat16)
+        pair_buf[layer, place, 0] = query
+        pair_buf[layer, place, 1] = key
+        if layer == 0:
+            norm_copy.wait()
+            pl.semaphore_wait(barrier, n - 1)
+        pair_copies = to_group(pair_buf.at[layer], pair_send.at[layer], pair_recv.at[layer])
+        if layer == 0:
+            norm_copies = to_group(norm_buf, norm_send, norm_recv)
+        both = lax.dot_general(
+            normed,
+            weights[layer, 2 * ncols : 4 * ncols],
+            NT,
+            preferred_element_type=jnp.float32,
+        )
+        value = both[:, :ncols].astype(jnp.bfloat16).astype(jnp.float32)
+        outgate = both[:, ncols:].astype(jnp.bfloat16).astype(jnp.float32)
+        gates = lax.dot_general(
+            normed, gate_buf[layer], NT, preferred_element_type=jnp.float32
+        )
+        in_gate = gates[:, :heads]
+        forget = gates[:, heads:] + bias_buf[pl.ds(layer, 1), :]
+        log_forget = jnp.minimum(forget, 0.0) - jnp.log1p(jnp.exp(-jnp.abs(forget)))
+        old_stab = stab_buf[layer].T
+        next_stab = jnp.maximum(log_forget + old_stab, in_gate)
+        new_stab[layer] = next_stab.T
+        mine = lax.broadcasted_iota(jnp.int32, (batch, heads), 1) == head
+
+        def pick(entry):
+            return jnp.sum(jnp.where(mine, entry, 0.0), axis=-1, keepdims=True)
+
+        my_stab = pick(next_stab)
+        my_decay = jnp.exp(pick(log_forget + old_stab) - my_stab)
+        my_weight = jnp.exp(pick(in_gate) - my_stab)
+        new_norm[layer] = my_decay * norm_buf[place, layer] + my_weight * key.astype(jnp.float32)
+        weighted = my_weight * value
+        wv_buf[layer] = weighted
+        decay_buf[layer] = jnp.broadcast_to(my_decay, (batch, ncols))
+        gate = jax.nn.sigmoid(outgate)
+
+        finish_group(pair_copies, pair_buf.at[layer], pair_recv.at[layer])
+        if layer == 0:
+            finish_group(norm_copies, norm_buf, norm_recv)
+        q_head = jnp.concatenate([pair_buf[layer, j, 0] for j in range(group)], axis=1)
+        q_head = q_head.astype(jnp.float32)
+        k_head = jnp.concatenate([pair_buf[layer, j, 1] for j in range(group)], axis=1)
+        k_head = k_head.astype(jnp.float32)
+        n_head = jnp.concatenate([norm_buf[j, layer] for j in range(group)], axis=1)
+        key_buf[layer] = k_head
+        denom = jnp.sum(
+            q_head * (my_decay * n_head + my_weight * k_head), axis=-1, keepdims=True
+        )
+        inner = jnp.sum(q_head * k_head, axis=-1, keepdims=True)
+
+        def read_rows(c, start, layer=layer):
+            queries = jnp.concatenate(
+                [pair_buf[layer, j, 0, pl.ds(start, rows), :] for j in range(group)], axis=1
+            )
+            row = lax.broadcasted_iota(jnp.int32, (rows, ncols), 0)
+            total = jnp.zeros((rows, ncols), jnp.float32)
+            for b in range(rows):
+                block = cell_buf[layer, start + b].astype(jnp.bfloat16)
+                product = lax.dot_general(
+                    queries, block, NT, preferred_element_type=jnp.float32
+                )
+                total = jnp.where(row == b, product, total)
+            numer_buf[pl.ds(start, rows), :] = total
+
+        for c in range(CELL_CHUNKS):
+            cell_copies[layer][c].wait()
+            read_rows(c, c * rows)
+        numer = my_decay * numer_buf[...] + weighted * inner
+        readout = numer / jnp.maximum(jnp.abs(denom), jnp.exp(-my_stab))
+        branch_buf[layer, me] = (gate * readout).astype(jnp.bfloat16)
+        branch_copies = to_all(
+            branch_buf.at[layer], gather_send.at[layer, 0], gather_recv.at[layer, 0]
+        )
+
+        weight_copies[layer][4].wait()
+        finish_all(branch_copies, branch_buf.at[layer], gather_recv.at[layer, 0])
+        branch = jnp.concatenate([branch_buf[layer, d] for d in range(n)], axis=1)
+        summed = lax.dot_general(
+            branch,
+            weights[layer, 4 * ncols : 5 * ncols],
+            NT,
+            preferred_element_type=jnp.float32,
+        )
+        result = (own + summed).astype(jnp.bfloat16)
+        own = result.astype(jnp.float32)
+        if layer + 1 < layers:
+            result_buf[layer, me] = result
+            result_copies = to_all(
+                result_buf.at[layer], gather_send.at[layer, 1], gather_recv.at[layer, 1]
+            )
+            finish_all(result_copies, result_buf.at[layer], gather_recv.at[layer, 1])
+        else:
+            mixed[...] = result
+
+
+def fused_body(n, *args):
+    (tokens, norm_gain, w_query, _, _, _, w_gates, bias_forget, _, cell, norm_vec, stab) = args
+    layers, batch, ncols, dh = cell.shape
+    width = tokens.shape[1]
+    group = dh // ncols
+    w_gates = jnp.swapaxes(w_gates, 1, 2)
+    stab = jnp.swapaxes(stab, 1, 2)
+    args = args[:6] + (w_gates,) + args[7:11] + (stab,)
+    args = [pltpu.with_memory_space_constraint(arg, pltpu.HBM) for arg in args]
+    bf16, f32 = jnp.bfloat16, jnp.float32
+    vmem = pl.BlockSpec(memory_space=pltpu.VMEM)
+    dma = pltpu.SemaphoreType.DMA
+    mixed, held, new_norm, new_stab, weighted, keys, decay = pl.pallas_call(
+        functools.partial(fused_kernel, n, group),
+        out_shape=(
+            jax.ShapeDtypeStruct((batch, ncols), bf16),
+            pltpu.VMEM(cell.shape, f32),
+            jax.ShapeDtypeStruct(norm_vec.shape, f32),
+            jax.ShapeDtypeStruct(stab.shape, f32),
+            jax.ShapeDtypeStruct((layers, batch, ncols), f32),
+            jax.ShapeDtypeStruct((layers, batch, dh), f32),
+            jax.ShapeDtypeStruct((layers, batch, ncols), f32),
+        ),
+        in_specs=[pl.BlockSpec(memory_space=pltpu.HBM)] * len(args),
+        out_specs=(vmem,) * 7,
+        scratch_shapes=[
+            pltpu.VMEM(tokens.shape, bf16),
+            pltpu.VMEM(norm_gain.shape, f32),
+            pltpu.VMEM((layers, 5 * ncols, width), bf16),
+            pltpu.VMEM(w_gates.shape, bf16),
+            pltpu.VMEM(bias_forget.shape, f32),
+            pltpu.VMEM(stab.shape, f32),
+            pltpu.VMEM((group,) + norm_vec.shape, f32),
+            pltpu.VMEM((layers, group, 2, batch, ncols), bf16),
+            pltpu.VMEM((layers, n, batch, ncols), bf16),
+            pltpu.VMEM((layers, n, batch, ncols), bf16),
+            pltpu.VMEM((batch, ncols), f32),
+            dma((6,)),
+            dma((layers, 5)),
+            dma((layers, CELL_CHUNKS)),
+            dma((group,)),
+            dma((group,)),
+            dma((layers, group)),
+            dma((layers, group)),
+            dma((layers, 2, n)),
+            dma((layers, 2, n)),
+        ],
+        compiler_params=pltpu.CompilerParams(
+            collective_id=0, has_side_effects=True, vmem_limit_bytes=VMEM_LIMIT
+        ),
+        name="cells",
+    )(*args)
+    new_cell = (
+        decay[:, :, :1, None] * held + weighted[:, :, :, None] * keys[:, :, None, :]
+    )
+    return mixed, new_cell, new_norm, jnp.swapaxes(new_stab, 1, 2)
+
+
+VMEM_LIMIT = 24 * 2**20
+
+
+def whole_body(*args):
+    n = lax.axis_size("tp")
+    _, batch, ncols, dh = args[9].shape
+    if ncols % 128 == 0 and dh % ncols == 0 and batch % (16 * CELL_CHUNKS) == 0:
+        return fused_body(n, *args)
+    return body(*args)
+
+
 def solution(mesh):
     return jax.shard_map(
-        body,
+        whole_body,
         mesh=mesh,
         in_specs=(
             P("grp", None),

time: 112 us -> 48 us (0.43)
  blocking collectives: 61 us -> 0 us
  Pallas kernels: 0 us -> 38.2 us
  matrix products: 27.1 us -> 0 us
  other arithmetic: 18.6 us -> 7.07 us
  starting transfers between devices: 2.11 us -> 0 us
    all_gather x3 -> x0, blocking collectives: 61 us -> none  [the longest x2 42.9 us: one_cell(): summed = project(lax.all_gather(branch, 'tp', axis=1, tiled=True), w_proj)]
    pallas_call x0 -> x1, Pallas kernels: none -> 38.2 us  [fused_body(): pl.pallas_call(functools.partial(fused_kernel, n, group), out_shape=(jax....]
    dot_general x14 -> x0, matrix products: 27.1 us -> none  [the longest x2 13.9 us: one_cell(): jnp.einsum('bk,bek->be', q_head.astype(jnp.float32), new_cell, precision=...]
    another operation x11 -> x0, other arithmetic: 9.64 us -> none  [the longest x7 9.6 us: body(): return (result, jnp.stack(cells), jnp.stack(norms), jnp.stack(stabs))]
    ppermute x6 -> x0, starting transfers between devices: 2.11 us -> none  [from_partner(): return lax.ppermute(value, axis, pairs)]
    add x1, other arithmetic: 5.09 us -> 7.07 us  [fused_body(): decay[:, :, :1, None] * held + weighted[:, :, :, None] * keys[:, :, None, :]]
    convert_element_type x9 -> x0, other arithmetic: 1.89 us -> none  [the longest x2 1.85 us: one_cell(): cur_f = current.astype(jnp.float32)]
    unnamed x28 -> x3, local copies, waits for them, and re-layouts: 0.07 us -> 1.83 us
  transfers between devices with their start and end apart: 6 -> 0, of which waited for: 0 -> 0; matrix products, arithmetic and copies ran while one was open for 14% -> 0% of each run, Pallas kernels for 0% -> 0%
where the time goes in v1:
time: 48 us; the launch traced here: 47.8 us
  Pallas kernels  38.2 us (80%)
  other arithmetic  7.07 us (15%)
  local copies, waits for them, and re-layouts  1.92 us (4%)
  between operations  0.65 us (1%)
    pallas_call x1, Pallas kernels, fused_body(): pl.pallas_call(functools.partial(fused_kernel, n, group), out_shape=(jax....  38.2 us
    add x1, other arithmetic, fused_body(): decay[:, :, :1, None] * held + weighted[:, :, :, None] * keys[:, :, None, :]  7.07 us
    unnamed x3, local copies, waits for them, and re-layouts  1.83 us

profile of v1, /device:TPU:0, one launch (start us, length us, event | category | flops | bytes accessed | tf_op | source)
XLA Modules:
  0.0 47.8 jit_solution(1943042857834189629)
XLA Ops:
  0.6 38.2 %cells.1 = (bf16[64,128]{1,0:T(8,128)(2,1)S(1)}, f32[2,64,128,256]{3,2,1,0:T(8,128)S(1)}, f32[2,64,128]{2,1,0:T(8,128)S(1)}, f32[2,8,64]{2,1,0:T(8,128)S(1)}, f3...) custom-call(bf16[64,2048]{1,0:T(8,128)(2,1)} %tokens.1, f32[2,2048]{1,0:T(2,128)} %norm_gain.1, ...), custom_call_target="tpu_custom_call" | custom-call | tf_op jit(solution)/shard_map/cells/pallas_call | solution.py:429
  38.8 0.1 slice_reduce_fusion
  38.9 7.1 %multiply_add_fusion = f32[2,64,128,256]{3,2,1,0:T(8,128)} fusion(f32[2,64,128,256]{3,2,1,0:T(8,128)S(1)} %get-tuple-element.13, f32[2,64,256]{2,1,0:T(8,128)S(1)} %get-tuple-element.15, f32[2,64,128]{2,1,0:T(8,128)S(1)} %get-tuple-element.14, f32[2,64]{1,0:T(2,128)S(1)} %slice_reduce_fusion), kind=kLoop, calls=%fused_computation | loop fusion | flops 12582912 | bytes 33751552 | tf_op jit(solution)/shard_map/add | solution.py:470
  46.0 0.6 %copy.19 = bf16[64,128]{1,0:T(8,128)(2,1)} copy(bf16[64,128]{1,0:T(8,128)(2,1)S(1)} %get-tuple-element.22) | data formatting | bytes 32768
  46.6 0.6 %copy.20 = f32[2,64,128]{2,1,0:T(8,128)} copy(f32[2,64,128]{2,1,0:T(8,128)S(1)} %get-tuple-element.24) | data formatting | bytes 131072
  47.2 0.6 %copy.21 = f32[2,64,8]{1,2,0:T(8,128)} copy(f32[2,64,8]{1,2,0:T(8,128)S(1)} %bitcast.3) | data formatting | bytes 8192

commit v2 on v1

--- a/solution.py
+++ b/solution.py
@@ -234,13 +234,16 @@
     names = [w_query, w_key, w_value, w_outgate, w_proj]
     weight_copies = [[None] * 5 for _ in range(layers)]
     cell_copies = [[None] * CELL_CHUNKS for _ in range(layers)]
-    for layer in range(layers):
+
+    def fetch_weights(layer):
         for i in range(4):
             weight_copies[layer][i] = fetch(
                 names[i].at[layer],
                 weights.at[layer, pl.ds(i * ncols, ncols)],
                 weight_sem.at[layer, i],
             )
+
+    def fetch_cell(layer):
         for c in range(CELL_CHUNKS):
             part = pl.ds(c * rows, rows)
             cell_copies[layer][c] = fetch(
@@ -251,6 +254,8 @@
             weights.at[layer, pl.ds(4 * ncols, ncols)],
             weight_sem.at[layer, 4],
         )
+
+    fetch_weights(0)
 
     def to_group(source, send, recv):
         copies = []
@@ -273,25 +278,41 @@
             pltpu.make_async_copy(source.at[origin], source.at[origin], recv.at[i]).wait()
             copy.wait_send()
 
+    chips = n // 2
+    core = lax.rem(me, 2)
+    chip = lax.div(me, 2)
+
+    def push(buffer, at, target, send, recv):
+        copy = pltpu.make_async_remote_copy(
+            src_ref=buffer.at[at],
+            dst_ref=buffer.at[at],
+            send_sem=send,
+            recv_sem=recv,
+            device_id={"tp": target},
+            device_id_type=pl.DeviceIdType.MESH,
+        )
+        copy.start()
+        return copy
+
     def to_all(buffer, send, recv):
-        copies = []
-        for i in range(1, n):
-            copy = pltpu.make_async_remote_copy(
-                src_ref=buffer.at[me],
-                dst_ref=buffer.at[me],
-                send_sem=send.at[i],
-                recv_sem=recv.at[i],
-                device_id={"tp": lax.rem(me + i, n)},
-                device_id_type=pl.DeviceIdType.MESH,
-            )
-            copy.start()
-            copies.append(copy)
+        copies = [
+            push(buffer, me, lax.rem(chip + i, chips) * 2 + core, send.at[0, i], recv.at[0, i])
+            for i in range(1, chips)
+        ]
+        copies.append(push(buffer, me, chip * 2 + 1 - core, send.at[1, 0], recv.at[1, 0]))
         return copies
 
-    def finish_all(copies, buffer, recv):
-        for i, copy in enumerate(copies, 1):
-            origin = lax.rem(me + n - i, n)
-            pltpu.make_async_copy(buffer.at[origin], buffer.at[origin], recv.at[i]).wait()
+    def finish_all(copies, buffer, send, recv):
+        for i in range(1, chips):
+            origin = lax.rem(chip + chips - i, chips) * 2 + core
+            pltpu.make_async_copy(buffer.at[origin], buffer.at[origin], recv.at[0, i]).wait()
+            copies.append(
+                push(buffer, origin, chip * 2 + 1 - core, send.at[1, i], recv.at[1, i])
+            )
+        for i in range(chips):
+            origin = lax.rem(chip + chips - i, chips) * 2 + 1 - core
+            pltpu.make_async_copy(buffer.at[origin], buffer.at[origin], recv.at[1, i]).wait()
+        for copy in copies:
             copy.wait_send()
 
     for copy in small:
@@ -311,6 +332,8 @@
         )
         for i in range(4):
             weight_copies[layer][i].wait()
+        if layer == 0:
+            fetch_cell(layer)
         both = lax.dot_general(
             normed, weights[layer, : 2 * ncols], NT, preferred_element_type=jnp.float32
         )
@@ -392,9 +415,17 @@
         branch_copies = to_all(
             branch_buf.at[layer], gather_send.at[layer, 0], gather_recv.at[layer, 0]
         )
+        if layer + 1 < layers:
+            fetch_weights(layer + 1)
+            fetch_cell(layer + 1)
 
         weight_copies[layer][4].wait()
-        finish_all(branch_copies, branch_buf.at[layer], gather_recv.at[layer, 0])
+        finish_all(
+            branch_copies,
+            branch_buf.at[layer],
+            gather_send.at[layer, 0],
+            gather_recv.at[layer, 0],
+        )
         branch = jnp.concatenate([branch_buf[layer, d] for d in range(n)], axis=1)
         summed = lax.dot_general(
             branch,
@@ -409,7 +440,12 @@
             result_copies = to_all(
                 result_buf.at[layer], gather_send.at[layer, 1], gather_recv.at[layer, 1]
             )
-            finish_all(result_copies, result_buf.at[layer], gather_recv.at[layer, 1])
+            finish_all(
+                result_copies,
+                result_buf.at[layer],
+                gather_send.at[layer, 1],
+                gather_recv.at[layer, 1],
+            )
         else:
             mixed[...] = result
 
@@ -458,8 +494,8 @@
             dma((group,)),
             dma((layers, group)),
             dma((layers, group)),
-            dma((layers, 2, n)),
-            dma((layers, 2, n)),
+            dma((layers, 2, 2, n // 2)),
+            dma((layers, 2, 2, n // 2)),
         ],
         compiler_params=pltpu.CompilerParams(
             collective_id=0, has_side_effects=True, vmem_limit_bytes=VMEM_LIMIT
@@ -469,7 +505,32 @@
     new_cell = (
         decay[:, :, :1, None] * held + weighted[:, :, :, None] * keys[:, :, None, :]
     )
+    mixed, new_norm, new_stab = write_small(mixed, new_norm, new_stab)
     return mixed, new_cell, new_norm, jnp.swapaxes(new_stab, 1, 2)
+
+
+def write_kernel(*refs):
+    half = len(refs) // 2
+    sems = refs[-1]
+    copies = [
+        pltpu.make_async_copy(refs[i], refs[half + i], sems.at[i]) for i in range(half)
+    ]
+    for copy in copies:
+        copy.start()
+    for copy in copies:
+        copy.wait()
+
+
+def write_small(*arrays):
+    return pl.pallas_call(
+        write_kernel,
+        out_shape=[jax.ShapeDtypeStruct(x.shape, x.dtype) for x in arrays],
+        in_specs=[pl.BlockSpec(memory_space=pltpu.VMEM)] * len(arrays),
+        out_specs=[pl.BlockSpec(memory_space=pltpu.HBM)] * len(arrays),
+        scratch_shapes=[pltpu.SemaphoreType.DMA((len(arrays),))],
+        compiler_params=pltpu.CompilerParams(vmem_limit_bytes=2**20),
+        name="write",
+    )(*arrays)
 
 
 VMEM_LIMIT = 24 * 2**20
@@ -478,7 +539,7 @@
 def whole_body(*args):
     n = lax.axis_size("tp")
     _, batch, ncols, dh = args[9].shape
-    if ncols % 128 == 0 and dh % ncols == 0 and batch % (16 * CELL_CHUNKS) == 0:
+    if n % 2 == 0 and ncols % 128 == 0 and dh % ncols == 0 and batch % (16 * CELL_CHUNKS) == 0:
         return fused_body(n, *args)
     return body(*args)
 

time: 48 us -> 41.2 us (0.86)
  Pallas kernels: 38.2 us -> 33.3 us
  local copies, waits for them, and re-layouts: 1.92 us -> 0.09 us
    pallas_call x1, Pallas kernels: 38.2 us -> 32.6 us  [fused_body(): pl.pallas_call(functools.partial(fused_kernel, n, group), out_shape=(jax....]
    unnamed x3 -> x0, local copies, waits for them, and re-layouts: 1.83 us -> none
    pallas_call x0 -> x1, Pallas kernels: none -> 0.67 us  [write_small(): pl.pallas_call(write_kernel, out_shape=[jax.ShapeDtypeStruct(x.shape, x.d...]
where the time goes in v2:
time: 41.2 us; the launch traced here: 41.1 us
  Pallas kernels  33.3 us (81%)
  other arithmetic  7.07 us (17%)
  between operations  0.65 us (2%)
    pallas_call x1, Pallas kernels, fused_body(): pl.pallas_call(functools.partial(fused_kernel, n, group), out_shape=(jax....  32.6 us
    add x1, other arithmetic, fused_body(): decay[:, :, :1, None] * held + weighted[:, :, :, None] * keys[:, :, None, :]  7.07 us

profile of v2, /device:TPU:0, one launch (start us, length us, event | category | flops | bytes accessed | tf_op | source)
XLA Modules:
  0.0 41.1 jit_solution(11256401918709460468)
XLA Ops:
  0.6 32.6 %cells.1 = (bf16[64,128]{1,0:T(8,128)(2,1)S(1)}, f32[2,64,128,256]{3,2,1,0:T(8,128)S(1)}, f32[2,64,128]{2,1,0:T(8,128)S(1)}, f32[2,8,64]{2,1,0:T(8,128)S(1)}, f3...) custom-call(bf16[64,2048]{1,0:T(8,128)(2,1)} %tokens.1, f32[2,2048]{1,0:T(2,128)} %norm_gain.1, ...), custom_call_target="tpu_custom_call" | custom-call | tf_op jit(solution)/shard_map/cells/pallas_call | solution.py:465
  33.2 0.7 %write.1 = (bf16[64,128]{1,0:T(8,128)(2,1)}, f32[2,64,128]{2,1,0:T(8,128)}, f32[2,8,64]{2,1,0:T(8,128)}) custom-call(bf16[64,128]{1,0:T(8,128)(2,1)S(1)} %get-tuple-element.14.refs_0_, f32[2,64,128]{2,1,0:T(8,128)S(1)} %get-tuple-element.15.refs_1_, f32[2,8,64]{2,1,0:T(8,128)S(1)} %get-tuple-element.16.refs_2_), custom_call_target="tpu_custom_call" | custom-call | tf_op jit(solution)/shard_map/write/pallas_call | solution.py:525
  33.9 0.1 slice_reduce_fusion
  34.0 7.1 %multiply_add_fusion = f32[2,64,128,256]{3,2,1,0:T(8,128)} fusion(f32[2,64,128,256]{3,2,1,0:T(8,128)S(1)} %get-tuple-element.19, f32[2,64,256]{2,1,0:T(8,128)S(1)} %get-tuple-element.21, f32[2,64,128]{2,1,0:T(8,128)S(1)} %get-tuple-element.20, f32[2,64]{1,0:T(2,128)S(1)} %slice_reduce_fusion), kind=kLoop, calls=%fused_computation | loop fusion | flops 12582912 | bytes 33751552 | tf_op jit(solution)/shard_map/add | solution.py:506
